TPU v7x, 32 devices: a whole 2x2x4 slice. The times are simulated.
32 devices in a mesh: grp: 2 (over y), ep: 4 (over z), tp: 4 (over x, core).
Axes of the slice: x: 2, y: 2, z: 4, core: 2. Of those that a mesh axis runs over, the one named last changes fastest.
Arguments:
- mixer_input: bfloat16 [4096, 2048], P(('grp', 'ep', 'tp')), parts along dimension 0, may hold values from -8 to 8
- forget_cumsum: float32 [8, 4096], P('tp', 'grp'), parts along dimension 1, may hold values from -259 to 0, as said below
- mixer_gain: float32 [2048], replicated, may hold values from 0.1 to 1.9
- query_weight: bfloat16 [2048, 1024], P(None, 'tp'), may hold values from -6 to 6
- key_weight: bfloat16 [2048, 1024], P(None, 'tp'), may hold values from -6 to 6
- value_weight: bfloat16 [2048, 1024], P(None, 'tp'), may hold values from -0.125 to 0.125
- out_weight: bfloat16 [1024, 2048], P('tp'), may hold values from -0.1875 to 0.1875
- post_gain: float32 [2048], replicated, may hold values from 0.1 to 1.9
- expert_input: bfloat16 [4096, 2048], P(('grp', 'ep', 'tp')), parts along dimension 0, may hold values from -6 to 6
- expert_gain: float32 [2048], replicated, may hold values from 0.1 to 1.9
- routes: int32 [4096, 2], P(('grp', 'ep', 'tp')), parts along dimension 0, may hold values from 0 to 3, all different within a row; in each aligned block of 128 rows (0 to 127, 128 to 255, ...) at most 72 rows name the same one
- route_weight: float32 [4096, 2], P(('grp', 'ep', 'tp')), parts along dimension 0, may hold values from 0.2 to 1
- expert_gate: bfloat16 [4, 2048, 2048], P('ep', None, 'tp'), may hold values from -0.125 to 0.125
- expert_upward: bfloat16 [4, 2048, 2048], P('ep', None, 'tp'), may hold values from -0.125 to 0.125
- expert_down: bfloat16 [4, 2048, 2048], P('ep', 'tp'), may hold values from -0.125 to 0.125
Outputs:
- mixer_output: bfloat16 [4096, 2048], P(('grp', 'ep', 'tp')), parts along dimension 0
- expert_output: bfloat16 [4096, 2048], P(('grp', 'ep', 'tp')), parts along dimension 0
There are 2 independent parts, one for each index of `grp`. A program takes and returns all parts, laid end to end along the dimension named above; an argument that names none is the same for every part. Nothing has to cross between parts.
Inputs may be any that keep to these rules, and one draw needn't show every extreme that they name: `forget_cumsum`: each head's row never rises along positions. `routes`: A row names 2 different experts. Within the rows of one device (aligned blocks of 128 rows) no expert is named by more than 72 rows, and in every draw some expert is named by exactly 72 rows of some block.
All inputs are finite; a program needn't handle non-finite values.
Results may differ from a plain program's by a relative error of at most 0.012.
Values may be sent and summed in bfloat16 or wider, within the bound.
A program may use at most 128 MiB of HBM per device.

v0:
```python
import jax
import jax.numpy as jnp
from jax import lax
from jax.sharding import PartitionSpec as P

EPS = 1e-06
MASKED = -1e30


def normalize(row_block, gain):
    values = row_block.astype(jnp.float32)
    inverse = lax.rsqrt(jnp.mean(values * values, axis=-1, keepdims=True) + EPS)
    return values * inverse * gain


def on_device(
    mixer_input,
    forget_cumsum,
    mixer_gain,
    query_weight,
    key_weight,
    value_weight,
    out_weight,
    post_gain,
    expert_input,
    expert_gain,
    routes,
    route_weight,
    expert_gate,
    expert_upward,
    expert_down,
):
    ep_count = lax.axis_size("ep")
    tp_count = lax.axis_size("tp")
    mix_rows = mixer_input.shape[0]
    feature_width = mixer_input.shape[1]
    heads_local = forget_cumsum.shape[0]
    head_width = query_weight.shape[1]
    head_dim = head_width // heads_local
    group_span = mix_rows * tp_count
    first_pos = lax.axis_index("ep") * group_span
    last_pos = first_pos + group_span - 1
    score_scale = head_dim ** (-0.5)
    normed = normalize(mixer_input, mixer_gain).astype(jnp.bfloat16)
    segment = lax.all_gather(normed, "tp", axis=0, tiled=True)
    products = [
        jnp.dot(segment, weight, preferred_element_type=jnp.float32)
        for weight in (query_weight, key_weight, value_weight)
    ]
    joined = jnp.concatenate(products, axis=1).astype(jnp.bfloat16)
    queries = joined[:, :head_width].reshape(group_span, heads_local, head_dim)
    key_rows = joined[:, head_width : 2 * head_width]
    value_rows = joined[:, 2 * head_width :]
    query_pos = first_pos + jnp.arange(group_span, dtype=jnp.int32)
    query_gate = lax.dynamic_slice_in_dim(forget_cumsum, first_pos, group_span, 1)

    def key_block(state, key_part, value_part, key_first):
        key_count = key_part.shape[0]

        def compute(current):
            running_max, running_sum, running_acc = current
            key_heads = key_part.reshape(key_count, heads_local, head_dim)
            value_heads = value_part.reshape(key_count, heads_local, head_dim)
            key_gate = lax.dynamic_slice_in_dim(forget_cumsum, key_first, key_count, 1)
            scores = (
                jnp.einsum("qhd,khd->hqk", queries, key_heads, preferred_element_type=jnp.float32)
                * score_scale
            )
            scores = scores + query_gate[:, :, None] - key_gate[:, None, :]
            key_pos = key_first + jnp.arange(key_count, dtype=jnp.int32)
            visible = (key_pos[None, :] <= query_pos[:, None])[None]
            scores = jnp.where(visible, scores, MASKED)
            new_max = jnp.maximum(running_max, jnp.max(scores, axis=-1))
            weights = jnp.where(visible, jnp.exp(scores - new_max[..., None]), 0.0)
            rescale = jnp.exp(running_max - new_max)
            running_sum = running_sum * rescale + jnp.sum(weights, axis=-1)
            running_acc = running_acc * rescale[..., None] + jnp.einsum(
                "hqk,khd->hqd",
                weights.astype(jnp.bfloat16),
                value_heads,
                preferred_element_type=jnp.float32,
            )
            return (new_max, running_sum, running_acc)

        def keep_state(current):
            return current

        return lax.cond(key_first > last_pos, keep_state, compute, state)

    initial = (
        jnp.full((heads_local, group_span), MASKED, jnp.float32),
        jnp.zeros((heads_local, group_span), jnp.float32),
        jnp.zeros((heads_local, group_span, head_dim), jnp.float32),
    )
    key_part = lax.all_gather(key_rows, "ep", axis=0, tiled=True)
    value_part = lax.all_gather(value_rows, "ep", axis=0, tiled=True)
    row_count = key_part.shape[0]
    block_size = 512
    block_count = row_count // block_size

    def advance_increment(block_index, current):
        offset = block_index * block_size
        return key_block(
            current,
            lax.dynamic_slice_in_dim(key_part, offset, block_size, 0),
            lax.dynamic_slice_in_dim(value_part, offset, block_size, 0),
            offset,
        )

    running_max, running_sum, running_acc = lax.fori_loop(
        0, block_count, advance_increment, initial
    )
    attended = (running_acc / running_sum[..., None]).astype(jnp.bfloat16)
    attended = attended.transpose(1, 0, 2).reshape(group_span, head_width)
    moe_rows, top_count = routes.shape
    experts_local = expert_gate.shape[0]
    experts_all = ep_count * experts_local
    capacity = (moe_rows * top_count * 9 + 8 * experts_all - 1) // (8 * experts_all)
    slots_all = experts_all * capacity
    normed_moe = normalize(expert_input, expert_gain).astype(jnp.bfloat16)
    flat_routes = routes.reshape(-1)
    member = (flat_routes[:, None] == jnp.arange(experts_all, dtype=jnp.int32)[None, :]).astype(
        jnp.int32
    )
    before = jnp.cumsum(member, axis=0) - member
    slot_rank = jnp.sum(before * member, axis=1)
    slot_index = (flat_routes * capacity + slot_rank).reshape(moe_rows, top_count)
    slot_ids = jnp.arange(slots_all, dtype=jnp.int32)
    choosers = [
        (slot_index[:, which][:, None] == slot_ids[None, :]).astype(jnp.bfloat16)
        for which in range(top_count)
    ]
    dispatch = choosers[0]
    which = 1
    dispatch = dispatch + choosers[which]
    outgoing = lax.dot_general(
        dispatch, normed_moe, (((0,), (0,)), ((), ())), preferred_element_type=jnp.float32
    ).astype(jnp.bfloat16)
    outgoing = outgoing.reshape(ep_count, experts_local, capacity, feature_width)
    copies = jnp.broadcast_to(
        outgoing[:, None], (ep_count, tp_count, experts_local, capacity, feature_width)
    )
    copies = copies.reshape(ep_count * tp_count, experts_local, capacity, feature_width)
    stacked = lax.all_to_all(copies, ("ep", "tp"), split_axis=0, concat_axis=0, tiled=True).reshape(
        ep_count, tp_count, experts_local, capacity, feature_width
    )
    shard_axis = 1
    expert_rows_count = ep_count * experts_local * capacity

    def expert_term(block_index):
        selected = lax.dynamic_index_in_dim(stacked, block_index, shard_axis, keepdims=False)
        gate_proj = jnp.einsum(
            "secd,edf->secf", selected, expert_gate, preferred_element_type=jnp.float32
        )
        upward = jnp.einsum(
            "secd,edf->secf", selected, expert_upward, preferred_element_type=jnp.float32
        )
        hidden = (jax.nn.silu(gate_proj) * upward).astype(jnp.bfloat16)
        result = jnp.einsum(
            "secf,efd->secd", hidden, expert_down, preferred_element_type=jnp.float32
        )
        return result.reshape(expert_rows_count, feature_width)

    selected = attended
    mixer_sum = lax.psum_scatter(
        jnp.dot(selected, out_weight, preferred_element_type=jnp.float32).astype(jnp.bfloat16),
        "tp",
        scatter_dimension=0,
        tiled=True,
    ).astype(jnp.float32)
    first_block = jnp.int32(0) // expert_rows_count
    pieces = [
        expert_term(first_block + offset)
        for offset in range(expert_rows_count * lax.axis_size("tp") // expert_rows_count)
    ]
    expert_sum = lax.psum_scatter(
        jnp.concatenate(pieces, axis=0).astype(jnp.bfloat16), "tp", scatter_dimension=0, tiled=True
    )
    mixer_output = normalize(mixer_sum, post_gain).astype(jnp.bfloat16)
    results = expert_sum.reshape(ep_count, experts_local, capacity, feature_width)
    returned = lax.all_to_all(results, "ep", split_axis=0, concat_axis=0, tiled=True).reshape(
        slots_all, feature_width
    )
    combined = jnp.zeros((moe_rows, feature_width), jnp.float32)
    for which in range(top_count):
        picked = jnp.dot(choosers[which], returned, preferred_element_type=jnp.float32)
        combined = combined + route_weight[:, which : which + 1] * picked
    expert_output = combined.astype(jnp.bfloat16)
    return (mixer_output, expert_output)


def solution(mesh):
    in_specs = (
        P(("grp", "ep", "tp"), None),
        P("tp", "grp"),
        P(),
        P(None, "tp"),
        P(None, "tp"),
        P(None, "tp"),
        P("tp", None),
        P(),
        P(("grp", "ep", "tp"), None),
        P(),
        P(("grp", "ep", "tp"), None),
        P(("grp", "ep", "tp"), None),
        P("ep", None, "tp"),
        P("ep", None, "tp"),
        P("ep", "tp", None),
    )
    out_specs = (P(("grp", "ep", "tp"), None), P(("grp", "ep", "tp"), None))
    return jax.shard_map(
        on_device, mesh=mesh, in_specs=in_specs, out_specs=out_specs, check_vma=False
    )
```

profile of v0, /device:TPU:0, one launch (start us, length us, event | category | flops | bytes accessed | tf_op | source)
XLA Modules:
  0.0 285.0 jit_solution(11052232415735645723)
XLA Ops:
  8.4 1.2 reduce-window.6
  11.0 1.2 fusion.97
  12.2 1.6 convolution_convert_fusion.1
  13.8 2.8 broadcast_in_dim.67
  16.6 7.6 %all-to-all-start = ((bf16[16,1,72,2048]{3,2,1,0:T(8,128)(2,1)}), bf16[16,1,72,2048]{3,2,1,0:T(8,128)(2,1)}, u32[]{:S(2)}, u32[]{:S(2)}) async-start(bf16[16,1,72,2048]{3,2,1,0:T(8,128)(2,1)} %bitcast.288), calls=%async_computation.1 | async-start | bytes 9437184 | tf_op jit(solution)/shard_map/all_to_all | solution.py:144
  24.4 1.0 fusion.93
  25.5 48.1 %all-gather.4.cloned.1.call-done = bf16[512,2048]{1,0:T(8,128)(2,1)} async-done(((bf16[128,2048]{1,0:T(8,128)(2,1)}), bf16[512,2048]{1,0:T(8,128)(2,1)}) %all-gather.4.cloned.1.call-update) | async-done | bytes 2097168 | tf_op jit(solution)/shard_map/all_gather | solution.py:45
  73.6 3.3 %convolution_convert_fusion.8 = bf16[512,256]{1,0:T(8,128)(2,1)} fusion(bf16[512,2048]{1,0:T(8,128)(2,1)} %all-gather.4.cloned.1.call-done, bf16[2048,256]{1,0:T(8,128)(2,1)} %param.23), kind=kOutput, calls=%fused_computation.73 | convolution fusion | flops 537001984 | bytes 3407872 | tf_op jit(solution)/shard_map/dot_general | solution.py:47
  77.0 3.0 %convolution_convert_fusion.6 = bf16[512,256]{1,0:T(8,128)(2,1)} fusion(bf16[512,2048]{1,0:T(8,128)(2,1)} %all-gather.4.cloned.1.call-done, bf16[2048,256]{1,0:T(8,128)(2,1)S(1)} %copy-done.7), kind=kOutput, calls=%fused_computation.71 | convolution fusion | flops 537001984 | bytes 3407872 | tf_op jit(solution)/shard_map/dot_general | solution.py:47
  80.1 47.6 %all-to-all-done = bf16[16,1,72,2048]{3,2,1,0:T(8,128)(2,1)} async-done(((bf16[16,1,72,2048]{3,2,1,0:T(8,128)(2,1)}), bf16[16,1,72,2048]{3,2,1,0:T(8,128)(2,1)}, u32[]{:S(2)}, u32[]{:S(2)}) %all-to-all-start) | async-done | bytes 4718624 | tf_op jit(solution)/shard_map/all_to_all | solution.py:144
  127.7 3.7 %fusion.31 = f32[4,1,72,512]{3,2,0,1:T(8,128)} fusion(bf16[1,2048,512]{2,1,0:T(8,128)(2,1)} %param.31, bf16[4,4,1,72,2048]{4,3,1,0,2:T(8,128)(2,1)} %bitcast.13), kind=kOutput, calls=%fused_computation.55 | convolution fusion | flops 603979776 | bytes 3866624 | tf_op jit(solution)/shard_map/secd,edf->secf/dot_general | solution.py:152
  131.4 2.9 %fusion.34 = f32[4,1,72,512]{3,2,0,1:T(8,128)} fusion(bf16[1,2048,512]{2,1,0:T(8,128)(2,1)S(1)} %copy-done.6, bf16[4,4,1,72,2048]{4,3,1,0,2:T(8,128)(2,1)} %bitcast.13), kind=kOutput, calls=%fused_computation.56 | convolution fusion | flops 603979776 | bytes 3866624 | tf_op jit(solution)/shard_map/secd,edf->secf/dot_general | solution.py:152
  134.3 2.9 %fusion.37 = f32[4,1,72,512]{3,2,0,1:T(8,128)} fusion(bf16[1,2048,512]{2,1,0:T(8,128)(2,1)S(1)} %copy-done.6, bf16[4,4,1,72,2048]{4,3,1,0,2:T(8,128)(2,1)} %bitcast.13), kind=kOutput, calls=%fused_computation.57 | convolution fusion | flops 603979776 | bytes 3866624 | tf_op jit(solution)/shard_map/secd,edf->secf/dot_general | solution.py:152
  137.1 3.6 %convolution_convert_fusion.5 = bf16[4,72,2048]{2,1,0:T(8,128)(2,1)S(1)} fusion(bf16[1,512,2048]{2,1,0:T(8,128)(2,1)S(1)} %copy-done, bf16[1,2048,512]{2,1,0:T(8,128)(2,1)} %param.32, bf16[4,4,1,72,2048]{4,3,1,0,2:T(8,128)(2,1)} %bitcast.13, f32[4,1,72,512]{3,2,0,1:T(8,128)} %fusion.31), kind=kOutput, calls=%fused_computation.24 | convolution fusion | flops 1209434112 | bytes 7143424 | tf_op jit(solution)/shard_map/secf,efd->secd/dot_general | solution.py:159
  140.8 4.6 %convolution_convert_fusion.4 = bf16[4,72,2048]{2,1,0:T(8,128)(2,1)} fusion(bf16[1,512,2048]{2,1,0:T(8,128)(2,1)S(1)} %copy-done, bf16[1,2048,512]{2,1,0:T(8,128)(2,1)} %param.32, bf16[4,4,1,72,2048]{4,3,1,0,2:T(8,128)(2,1)} %bitcast.13, f32[4,1,72,512]{3,2,0,1:T(8,128)} %fusion.34), kind=kOutput, calls=%fused_computation.23 | convolution fusion | flops 1209434112 | bytes 7143424 | tf_op jit(solution)/shard_map/secf,efd->secd/dot_general | solution.py:159
  145.4 4.6 %convolution_convert_fusion.3 = bf16[4,72,2048]{2,1,0:T(8,128)(2,1)} fusion(bf16[1,512,2048]{2,1,0:T(8,128)(2,1)S(1)} %copy-done, bf16[1,2048,512]{2,1,0:T(8,128)(2,1)} %param.32, bf16[4,4,1,72,2048]{4,3,1,0,2:T(8,128)(2,1)} %bitcast.13, f32[4,1,72,512]{3,2,0,1:T(8,128)} %fusion.37), kind=kOutput, calls=%fused_computation.22 | convolution fusion | flops 1209434112 | bytes 7143424 | tf_op jit(solution)/shard_map/secf,efd->secd/dot_general | solution.py:159
  150.0 3.6 %fusion.40 = f32[4,1,72,512]{3,2,0,1:T(8,128)} fusion(bf16[1,2048,512]{2,1,0:T(8,128)(2,1)} %param.31, bf16[4,4,1,72,2048]{4,3,1,0,2:T(8,128)(2,1)} %bitcast.13), kind=kOutput, calls=%fused_computation.58 | convolution fusion | flops 603979776 | bytes 3866624 | tf_op jit(solution)/shard_map/secd,edf->secf/dot_general | solution.py:152
  153.6 4.6 %convolution_convert_fusion.2 = bf16[4,72,2048]{2,1,0:T(8,128)(2,1)} fusion(bf16[1,512,2048]{2,1,0:T(8,128)(2,1)S(1)} %copy-done, bf16[1,2048,512]{2,1,0:T(8,128)(2,1)} %param.32, bf16[4,4,1,72,2048]{4,3,1,0,2:T(8,128)(2,1)} %bitcast.13, f32[4,1,72,512]{3,2,0,1:T(8,128)} %fusion.40), kind=kOutput, calls=%fused_computation.21 | convolution fusion | flops 1209434112 | bytes 7143424 | tf_op jit(solution)/shard_map/secf,efd->secd/dot_general | solution.py:159
  158.2 3.9 %pad_maximum_fusion = bf16[1152,2048]{1,0:T(8,128)(2,1)} fusion(bf16[288,2048]{1,0:T(8,128)(2,1)} %bitcast.297, bf16[288,2048]{1,0:T(8,128)(2,1)} %bitcast.296, bf16[288,2048]{1,0:T(8,128)(2,1)} %bitcast.295, bf16[288,2048]{1,0:T(8,128)(2,1)S(1)} %bitcast.294), kind=kLoop, calls=%fused_computation.18 | loop fusion | flops 18874368 | bytes 9437184 | tf_op jit(solution)/shard_map/concatenate | solution.py:177
  162.8 2.6 convolution_convert_fusion.7
  165.6 2.3 copy.75
  167.9 2.3 copy.77
  170.2 3.8 %while.18 = (s32[]{:T(128)}, f32[2,512]{1,0:T(2,128)S(1)}, f32[2,512]{1,0:T(2,128)S(1)}, f32[2,512,128]{2,1,0:T(8,128)S(1)}, s32[]{:T(128)}, /*index=5*/bf16[204...) while((s32[]{:T(128)}, f32[2,512]{1,0:T(2,128)S(1)}, ...), condition=%wide.region_6.7_spmd.clone, body=%wide.region_1.6_spmd.clone.sunk | while | flops 274729984 | bytes 10318161 | solution.py:110
  170.3 3.5 %conditional.3 = (f32[2,512]{1,0:T(2,128)S(1)}, f32[2,512]{1,0:T(2,128)S(1)}, f32[2,512,128]{2,1,0:T(8,128)S(1)}) conditional(s32[]{:T(128)} %convert_element_type.155, (s32[]{:T(128)}, s32[]{:T(128)}, bf16[2048,256]{0,1:T(8,128)(2,1)}, bf16[512,2,128]{2,0,1:T(8,128)(2,1)S(1)}, f32[2,512]{1,0:T(2,128)S(1)}, /*index=5*/f32[2,2048]{1,0:T(2,128)S(1)}, ...), branch_computations={%region_2.4_spmd, %region_5.5_spmd} | conditional | flops 274729984 | bytes 10307658 | solution.py:88
  170.3 1.1 constant_dynamic-slice_fusion.1
  174.3 3.4 %convolution_convert_fusion = bf16[512,2048]{1,0:T(8,128)(2,1)} fusion(bf16[512,256]{0,1:T(8,128)(2,1)S(1)} %bitcast.293, bf16[256,2048]{1,0:T(8,128)(2,1)} %param.25), kind=kOutput, calls=%fused_computation.19 | convolution fusion | flops 537919488 | bytes 3407872 | tf_op jit(solution)/shard_map/dot_general | solution.py:166
  177.7 62.1 %reduce-scatter.5.cloned.1.call-done = bf16[288,2048]{1,0:T(8,128)(2,1)} async-done(((bf16[1152,2048]{1,0:T(8,128)(2,1)}), bf16[288,2048]{1,0:T(8,128)(2,1)}) %reduce-scatter.5.cloned.1.call-update) | async-done | bytes 1179664 | tf_op jit(solution)/shard_map/reduce_scatter | solution.py:176
  239.8 4.6 %all-to-all-start.1 = ((bf16[4,1,72,2048]{3,2,1,0:T(8,128)(2,1)}), bf16[4,1,72,2048]{3,2,1,0:T(8,128)(2,1)S(1)}, u32[]{:S(2)}, u32[]{:S(2)}) async-start(bf16[4,1,72,2048]{3,2,1,0:T(8,128)(2,1)} %bitcast.298), calls=%async_computation.3 | async-start | bytes 2359296 | tf_op jit(solution)/shard_map/all_to_all | solution.py:181
  244.4 28.9 %reduce-scatter.3.cloned.1.call-done = bf16[128,2048]{1,0:T(8,128)(2,1)} async-done(((bf16[512,2048]{1,0:T(8,128)(2,1)}), bf16[128,2048]{1,0:T(8,128)(2,1)}) %reduce-scatter.3.cloned.1.call-update) | async-done | bytes 524304 | tf_op jit(solution)/shard_map/reduce_scatter | solution.py:165
  273.4 1.2 fusion.94
  274.6 2.0 fusion.96
  277.1 1.3 fusion.10
  (79 shorter events, 7.2 us)
Async XLA Ops:
  7.2 130.0 %copy-start = (bf16[1,512,2048]{2,1,0:T(8,128)(2,1)S(1)}, bf16[1,512,2048]{2,1,0:T(8,128)(2,1)}, u32[]{:S(2)}) copy-start(bf16[1,512,2048]{2,1,0:T(8,128)(2,1)} %param.33) | copy-start | bytes 6291460
  16.6 7.6 %copy-start.1 = (bf16[128,2048]{1,0:T(8,128)(2,1)S(1)}, bf16[128,2048]{1,0:T(8,128)(2,1)}, u32[]{:S(2)}) copy-start(bf16[128,2048]{1,0:T(8,128)(2,1)} %param.19) | copy-start | bytes 1572868
  16.6 7.8 %copy-start.3 = (f32[2048]{0:T(1024)S(1)}, f32[2048]{0:T(1024)}, u32[]{:S(2)}) copy-start(f32[2048]{0:T(1024)} %param.21) | copy-start | bytes 24580
  16.6 111.1 %all-to-all-start = ((bf16[16,1,72,2048]{3,2,1,0:T(8,128)(2,1)}), bf16[16,1,72,2048]{3,2,1,0:T(8,128)(2,1)}, u32[]{:S(2)}, u32[]{:S(2)}) async-start(bf16[16,1,72,2048]{3,2,1,0:T(8,128)(2,1)} %bitcast.288), calls=%async_computation.1 | async-start | bytes 9437184 | tf_op jit(solution)/shard_map/all_to_all | solution.py:144
  24.2 49.5 %all-gather.4.cloned.1.call-start = ((), (), s32[]{:S(2)}) async-start(), calls=%async_computation.4 | async-start | bytes 2621440 | tf_op jit(solution)/shard_map/all_gather | solution.py:45
  25.4 51.5 %copy-start.7 = (bf16[2048,256]{1,0:T(8,128)(2,1)S(1)}, bf16[2048,256]{1,0:T(8,128)(2,1)}, u32[]{:S(2)}) copy-start(bf16[2048,256]{1,0:T(8,128)(2,1)} %param.24) | copy-start | bytes 3145732
  25.5 140.1 %all-gather.6.cloned.1.call-start = ((), (), s32[]{:S(2)}) async-start(), calls=%async_computation.5 | async-start | bytes 1310720 | tf_op jit(solution)/shard_map/all_gather | solution.py:95
  76.9 91.0 %all-gather.8.cloned.1.call-start = ((), (), s32[]{:S(2)}) async-start(), calls=%async_computation.6 | async-start | bytes 1310720 | tf_op jit(solution)/shard_map/all_gather | solution.py:96
  80.0 159.8 %reduce-scatter.5.cloned.1.call-start = ((), (), s32[]{:S(2)}) async-start(), calls=%async_computation.8 | async-start | bytes 5898240 | tf_op jit(solution)/shard_map/reduce_scatter | solution.py:176
  127.7 3.7 %copy-start.6 = (bf16[1,2048,512]{2,1,0:T(8,128)(2,1)S(1)}, bf16[1,2048,512]{2,1,0:T(8,128)(2,1)}, u32[]{:S(2)}) copy-start(bf16[1,2048,512]{2,1,0:T(8,128)(2,1)} %param.31) | copy-start | bytes 6291460
  162.1 0.7 copy-start.2
  162.1 111.3 %reduce-scatter.3.cloned.1.call-start = ((), (), s32[]{:S(2)}) async-start(), calls=%async_computation.7 | async-start | bytes 2621440 | tf_op jit(solution)/shard_map/reduce_scatter | solution.py:165
  177.7 66.7 %copy-start.5 = (f32[128,2]{0,1:T(2,128)S(1)}, f32[128,2]{0,1:T(2,128)}, u32[]{:S(2)}) copy-start(f32[128,2]{0,1:T(2,128)} %param.30) | copy-start | bytes 3076
  177.7 96.9 %copy-start.4 = (f32[2048]{0:T(1024)S(1)}, f32[2048]{0:T(1024)}, u32[]{:S(2)}) copy-start(f32[2048]{0:T(1024)} %param.26) | copy-start | bytes 24580
  239.8 36.8 %all-to-all-start.1 = ((bf16[4,1,72,2048]{3,2,1,0:T(8,128)(2,1)}), bf16[4,1,72,2048]{3,2,1,0:T(8,128)(2,1)S(1)}, u32[]{:S(2)}, u32[]{:S(2)}) async-start(bf16[4,1,72,2048]{3,2,1,0:T(8,128)(2,1)} %bitcast.298), calls=%async_computation.3 | async-start | bytes 2359296 | tf_op jit(solution)/shard_map/all_to_all | solution.py:181
Sparse Core Ops, SparseCore 0:
  27.1 46.4 all-gather.3
  77.0 41.1 all-gather.5
  120.4 43.0 all-gather.7
  165.9 73.9 reduce-scatter.4
  242.2 31.1 reduce-scatter.2
where the time goes:
time: 286 us; the launch traced here: 285 us
  waiting for transfers between devices  187 us (65%)
  matrix products  47.8 us (17%)
  between operations  14 us (5%)
  starting transfers between devices  12.6 us (4%)
  other arithmetic  12.3 us (4%)
  local copies, waits for them, and re-layouts  11 us (4%)
    reduce_scatter x1, waiting for transfers between devices, on_device(): lax.psum_scatter(jnp.concatenate(pieces, axis=0).astype(jnp.bfloat16), 't...  62.1 us
    all_gather x1, waiting for transfers between devices, on_device(): segment = lax.all_gather(normed, 'tp', axis=0, tiled=True)  48.1 us
    all_to_all x1, waiting for transfers between devices, on_device(): lax.all_to_all(copies, ('ep', 'tp'), split_axis=0, concat_axis=0, tiled=T...  47.6 us
    reduce_scatter x1, waiting for transfers between devices, on_device(): lax.psum_scatter(jnp.dot(selected, out_weight, preferred_element_type=jnp...  28.9 us
    dot_general x4, matrix products, expert_term(): jnp.einsum('secf,efd->secd', hidden, expert_down, preferred_element_type=...  17.4 us
    dot_general x4, matrix products, expert_term(): jnp.einsum('secd,edf->secf', selected, expert_gate, preferred_element_typ...  13 us
    dot_general x3, matrix products, on_device(): jnp.dot(segment, weight, preferred_element_type=jnp.float32)  8.88 us
    all_to_all x1, starting transfers between devices, on_device(): lax.all_to_all(copies, ('ep', 'tp'), split_axis=0, concat_axis=0, tiled=T...  7.56 us
  transfers between devices with their start and end apart: 7, of which 4 were waited for; matrix products, arithmetic and copies ran while one was open for 21% of the time, Pallas kernels for 0%

commit v1 on v0

--- a/solution.py
+++ b/solution.py
@@ -42,7 +42,12 @@
     last_pos = first_pos + group_span - 1
     score_scale = head_dim ** (-0.5)
     normed = normalize(mixer_input, mixer_gain).astype(jnp.bfloat16)
-    segment = lax.all_gather(normed, "tp", axis=0, tiled=True)
+    ring = [normed]
+    for hop in range(3):
+        ring.append(lax.ppermute(ring[-1], "tp", [(dev, (dev + 1) % 4) for dev in range(4)]))
+    segment = jnp.roll(
+        jnp.concatenate(ring[::-1], axis=0), (lax.axis_index("tp") + 1) * ring[0].shape[0], axis=0
+    )
     products = [
         jnp.dot(segment, weight, preferred_element_type=jnp.float32)
         for weight in (query_weight, key_weight, value_weight)

time: 286 us -> 275 us (0.962)
  waiting for transfers between devices: 187 us -> 170 us
  local copies, waits for them, and re-layouts: 11 us -> 17.6 us
    ppermute x0 -> x3, waiting for transfers between devices: none -> 59.5 us  [on_device(): lax.ppermute(ring[-1], 'tp', [(dev, (dev + 1) % 4) for dev in range(4)])]
    all_gather x1 -> x0, waiting for transfers between devices: 48.1 us -> none  [on_device(): segment = lax.all_gather(normed, 'tp', axis=0, tiled=True)]
    all_to_all x1, waiting for transfers between devices: 47.6 us -> 14.9 us  [on_device(): lax.all_to_all(copies, ('ep', 'tp'), split_axis=0, concat_axis=0, tiled=T...]
    all_gather x1, waiting for transfers between devices: 0.02 us -> 13.6 us  [on_device(): key_part = lax.all_gather(key_rows, 'ep', axis=0, tiled=True)]
    reduce_scatter x1, waiting for transfers between devices: 62.1 us -> 52.7 us  [on_device(): lax.psum_scatter(jnp.concatenate(pieces, axis=0).astype(jnp.bfloat16), 't...]
    unnamed x20 -> x30, local copies, waits for them, and re-layouts: 6.17 us -> 12.7 us
  transfers between devices with their start and end apart: 7 -> 9, of which waited for: 4 -> 7; matrix products, arithmetic and copies ran while one was open for 21% -> 23% of each run, Pallas kernels for 0% -> 0%
where the time goes in v1:
time: 275 us; the launch traced here: 274 us
  waiting for transfers between devices  170 us (62%)
  matrix products  45.9 us (17%)
  local copies, waits for them, and re-layouts  17.6 us (6%)
  between operations  15.7 us (6%)
  starting transfers between devices  12.9 us (5%)
  other arithmetic  12 us (4%)
    ppermute x3, waiting for transfers between devices, on_device(): lax.ppermute(ring[-1], 'tp', [(dev, (dev + 1) % 4) for dev in range(4)])  59.5 us
    reduce_scatter x1, waiting for transfers between devices, on_device(): lax.psum_scatter(jnp.concatenate(pieces, axis=0).astype(jnp.bfloat16), 't...  52.7 us
    reduce_scatter x1, waiting for transfers between devices, on_device(): lax.psum_scatter(jnp.dot(selected, out_weight, preferred_element_type=jnp...  28.9 us
    dot_general x4, matrix products, expert_term(): jnp.einsum('secf,efd->secd', hidden, expert_down, preferred_element_type=...  17.4 us
    all_to_all x1, waiting for transfers between devices, on_device(): lax.all_to_all(copies, ('ep', 'tp'), split_axis=0, concat_axis=0, tiled=T...  14.9 us
    all_gather x1, waiting for transfers between devices, on_device(): key_part = lax.all_gather(key_rows, 'ep', axis=0, tiled=True)  13.6 us
    dot_general x4, matrix products, expert_term(): jnp.einsum('secd,edf->secf', selected, expert_gate, preferred_element_typ...  13 us
    unnamed x30, local copies, waits for them, and re-layouts  12.7 us
  transfers between devices with their start and end apart: 9, of which 7 were waited for; matrix products, arithmetic and copies ran while one was open for 23% of the time, Pallas kernels for 0%

profile of v1, /device:TPU:0, one launch (start us, length us, event | category | flops | bytes accessed | tf_op | source)
XLA Modules:
  0.0 274.1 jit_solution(2790966671490310777)
XLA Ops:
  13.0 1.6 convolution_convert_fusion.1
  14.7 2.8 %broadcast_in_dim.67 = bf16[4,4,72,2048]{3,2,1,0:T(8,128)(2,1)} broadcast(bf16[4,72,2048]{2,1,0:T(8,128)(2,1)S(1)} %bitcast.289), dimensions={0,2,3} | broadcast | bytes 5898240 | tf_op jit(solution)/shard_map/broadcast_in_dim | solution.py:145
  17.4 7.6 %all-to-all-start = ((bf16[16,1,72,2048]{3,2,1,0:T(8,128)(2,1)}), bf16[16,1,72,2048]{3,2,1,0:T(8,128)(2,1)}, u32[]{:S(2)}, u32[]{:S(2)}) async-start(bf16[16,1,72,2048]{3,2,1,0:T(8,128)(2,1)} %bitcast.285), calls=%async_computation.1 | async-start | bytes 9437184 | tf_op jit(solution)/shard_map/all_to_all | solution.py:149
  25.9 34.1 %collective-permute-done = bf16[128,2048]{1,0:T(8,128)(2,1)S(1)} collective-permute-done((bf16[128,2048]{1,0:T(8,128)(2,1)S(1)}, bf16[128,2048]{1,0:T(8,128)(2,1)S(1)}, u32[]{:S(2)}, u32[]{:S(2)}) %collective-permute-start) | collective-permute-done | bytes 524320 | tf_op jit(solution)/shard_map/ppermute | solution.py:47
  60.0 14.8 %collective-permute-done.1 = bf16[128,2048]{1,0:T(8,128)(2,1)} collective-permute-done((bf16[128,2048]{1,0:T(8,128)(2,1)S(1)}, bf16[128,2048]{1,0:T(8,128)(2,1)}, u32[]{:S(2)}, u32[]{:S(2)}) %collective-permute-start.1) | collective-permute-done | bytes 524320 | tf_op jit(solution)/shard_map/ppermute | solution.py:47
  74.8 10.6 %collective-permute-done.2 = bf16[128,2048]{1,0:T(8,128)(2,1)} collective-permute-done((bf16[128,2048]{1,0:T(8,128)(2,1)}, bf16[128,2048]{1,0:T(8,128)(2,1)}, u32[]{:S(2)}, u32[]{:S(2)}) %collective-permute-start.2) | collective-permute-done | bytes 524320 | tf_op jit(solution)/shard_map/ppermute | solution.py:47
  90.3 2.1 copy-done.3
  92.4 1.4 fusion.91
  93.9 3.0 %fusion.85 = bf16[512,256]{1,0:T(8,128)(2,1)} fusion(bf16[2048,256]{1,0:T(8,128)(2,1)S(1)} %copy-done.9, bf16[1024,2048]{1,0:T(8,128)(2,1)} %copy-done.3, s32[]{:T(128)S(6)} %select_n.53), kind=kOutput, calls=%fused_computation.77 | convolution fusion | flops 537001984 | bytes 3407876 | tf_op jit(solution)/shard_map/dot_general | solution.py:52
  97.0 14.9 %all-to-all-done = bf16[16,1,72,2048]{3,2,1,0:T(8,128)(2,1)} async-done(((bf16[16,1,72,2048]{3,2,1,0:T(8,128)(2,1)}), bf16[16,1,72,2048]{3,2,1,0:T(8,128)(2,1)}, u32[]{:S(2)}, u32[]{:S(2)}) %all-to-all-start) | async-done | bytes 4718624 | tf_op jit(solution)/shard_map/all_to_all | solution.py:149
  111.8 3.7 %fusion.37 = f32[4,1,72,512]{3,2,0,1:T(8,128)} fusion(bf16[1,2048,512]{2,1,0:T(8,128)(2,1)} %param.31, bf16[4,4,1,72,2048]{4,3,1,0,2:T(8,128)(2,1)} %bitcast.13), kind=kOutput, calls=%fused_computation.61 | convolution fusion | flops 603979776 | bytes 3866624 | tf_op jit(solution)/shard_map/secd,edf->secf/dot_general | solution.py:157
  115.5 2.9 %fusion.40 = f32[4,1,72,512]{3,2,0,1:T(8,128)} fusion(bf16[1,2048,512]{2,1,0:T(8,128)(2,1)S(1)} %copy-done.7, bf16[4,4,1,72,2048]{4,3,1,0,2:T(8,128)(2,1)} %bitcast.13), kind=kOutput, calls=%fused_computation.62 | convolution fusion | flops 603979776 | bytes 3866624 | tf_op jit(solution)/shard_map/secd,edf->secf/dot_general | solution.py:157
  118.4 2.9 %fusion.43 = f32[4,1,72,512]{3,2,0,1:T(8,128)} fusion(bf16[1,2048,512]{2,1,0:T(8,128)(2,1)S(1)} %copy-done.7, bf16[4,4,1,72,2048]{4,3,1,0,2:T(8,128)(2,1)} %bitcast.13), kind=kOutput, calls=%fused_computation.63 | convolution fusion | flops 603979776 | bytes 3866624 | tf_op jit(solution)/shard_map/secd,edf->secf/dot_general | solution.py:157
  121.3 3.6 %convolution_convert_fusion.5 = bf16[4,72,2048]{2,1,0:T(8,128)(2,1)S(1)} fusion(bf16[1,512,2048]{2,1,0:T(8,128)(2,1)S(1)} %copy-done, bf16[1,2048,512]{2,1,0:T(8,128)(2,1)} %param.32, bf16[4,4,1,72,2048]{4,3,1,0,2:T(8,128)(2,1)} %bitcast.13, f32[4,1,72,512]{3,2,0,1:T(8,128)} %fusion.37), kind=kOutput, calls=%fused_computation.24 | convolution fusion | flops 1209434112 | bytes 7143424 | tf_op jit(solution)/shard_map/secf,efd->secd/dot_general | solution.py:164
  124.8 4.6 %convolution_convert_fusion.4 = bf16[4,72,2048]{2,1,0:T(8,128)(2,1)} fusion(bf16[1,512,2048]{2,1,0:T(8,128)(2,1)S(1)} %copy-done, bf16[1,2048,512]{2,1,0:T(8,128)(2,1)} %param.32, bf16[4,4,1,72,2048]{4,3,1,0,2:T(8,128)(2,1)} %bitcast.13, f32[4,1,72,512]{3,2,0,1:T(8,128)} %fusion.40), kind=kOutput, calls=%fused_computation.23 | convolution fusion | flops 1209434112 | bytes 7143424 | tf_op jit(solution)/shard_map/secf,efd->secd/dot_general | solution.py:164
  129.5 4.6 %convolution_convert_fusion.3 = bf16[4,72,2048]{2,1,0:T(8,128)(2,1)} fusion(bf16[1,512,2048]{2,1,0:T(8,128)(2,1)S(1)} %copy-done, bf16[1,2048,512]{2,1,0:T(8,128)(2,1)} %param.32, bf16[4,4,1,72,2048]{4,3,1,0,2:T(8,128)(2,1)} %bitcast.13, f32[4,1,72,512]{3,2,0,1:T(8,128)} %fusion.43), kind=kOutput, calls=%fused_computation.22 | convolution fusion | flops 1209434112 | bytes 7143424 | tf_op jit(solution)/shard_map/secf,efd->secd/dot_general | solution.py:164
  134.1 3.6 %fusion.46 = f32[4,1,72,512]{3,2,0,1:T(8,128)} fusion(bf16[1,2048,512]{2,1,0:T(8,128)(2,1)} %param.31, bf16[4,4,1,72,2048]{4,3,1,0,2:T(8,128)(2,1)} %bitcast.13), kind=kOutput, calls=%fused_computation.64 | convolution fusion | flops 603979776 | bytes 3866624 | tf_op jit(solution)/shard_map/secd,edf->secf/dot_general | solution.py:157
  137.7 4.6 %convolution_convert_fusion.2 = bf16[4,72,2048]{2,1,0:T(8,128)(2,1)} fusion(bf16[1,512,2048]{2,1,0:T(8,128)(2,1)S(1)} %copy-done, bf16[1,2048,512]{2,1,0:T(8,128)(2,1)} %param.32, bf16[4,4,1,72,2048]{4,3,1,0,2:T(8,128)(2,1)} %bitcast.13, f32[4,1,72,512]{3,2,0,1:T(8,128)} %fusion.46), kind=kOutput, calls=%fused_computation.21 | convolution fusion | flops 1209434112 | bytes 7143424 | tf_op jit(solution)/shard_map/secf,efd->secd/dot_general | solution.py:164
  142.2 3.9 %pad_maximum_fusion = bf16[1152,2048]{1,0:T(8,128)(2,1)} fusion(bf16[288,2048]{1,0:T(8,128)(2,1)} %bitcast.294, bf16[288,2048]{1,0:T(8,128)(2,1)} %bitcast.293, bf16[288,2048]{1,0:T(8,128)(2,1)} %bitcast.292, bf16[288,2048]{1,0:T(8,128)(2,1)S(1)} %bitcast.291), kind=kLoop, calls=%fused_computation.18 | loop fusion | flops 18874368 | bytes 9437184 | tf_op jit(solution)/shard_map/concatenate | solution.py:182
  146.9 2.6 fusion.88
  149.7 2.3 copy.77
  152.0 13.6 %all-gather.3.cloned.1.call-done = bf16[2048,256]{1,0:T(8,128)(2,1)} async-done(((bf16[512,256]{1,0:T(8,128)(2,1)}), bf16[2048,256]{1,0:T(8,128)(2,1)}) %all-gather.3.cloned.1.call-update) | async-done | bytes 1048592 | tf_op jit(solution)/shard_map/all_gather | solution.py:100
  165.5 2.3 copy.75
  167.9 3.8 %while.18 = (s32[]{:T(128)}, f32[2,512]{1,0:T(2,128)S(1)}, f32[2,512]{1,0:T(2,128)S(1)}, f32[2,512,128]{2,1,0:T(8,128)S(1)}, s32[]{:T(128)}, /*index=5*/bf16[204...) while((s32[]{:T(128)}, f32[2,512]{1,0:T(2,128)S(1)}, ...), condition=%wide.region_6.7_spmd.clone, body=%wide.region_1.6_spmd.clone.sunk | while | flops 274729984 | bytes 10318161 | solution.py:115
  167.9 3.5 %conditional.3 = (f32[2,512]{1,0:T(2,128)S(1)}, f32[2,512]{1,0:T(2,128)S(1)}, f32[2,512,128]{2,1,0:T(8,128)S(1)}) conditional(s32[]{:T(128)} %convert_element_type.163, (s32[]{:T(128)}, s32[]{:T(128)}, bf16[2048,256]{0,1:T(8,128)(2,1)}, bf16[512,2,128]{2,0,1:T(8,128)(2,1)S(1)}, f32[2,512]{1,0:T(2,128)S(1)}, /*index=5*/f32[2,2048]{1,0:T(2,128)S(1)}, ...), branch_computations={%region_2.4_spmd, %region_5.5_spmd} | conditional | flops 274729984 | bytes 10307658 | solution.py:93
  172.0 3.4 %convolution_convert_fusion = bf16[512,2048]{1,0:T(8,128)(2,1)} fusion(bf16[512,256]{0,1:T(8,128)(2,1)S(1)} %bitcast.290, bf16[256,2048]{1,0:T(8,128)(2,1)} %param.25), kind=kOutput, calls=%fused_computation.19 | convolution fusion | flops 537919488 | bytes 3407872 | tf_op jit(solution)/shard_map/dot_general | solution.py:171
  175.4 52.7 %reduce-scatter.5.cloned.1.call-done = bf16[288,2048]{1,0:T(8,128)(2,1)} async-done(((bf16[1152,2048]{1,0:T(8,128)(2,1)}), bf16[288,2048]{1,0:T(8,128)(2,1)}) %reduce-scatter.5.cloned.1.call-update) | async-done | bytes 1179664 | tf_op jit(solution)/shard_map/reduce_scatter | solution.py:181
  228.0 4.6 %all-to-all-start.1 = ((bf16[4,1,72,2048]{3,2,1,0:T(8,128)(2,1)}), bf16[4,1,72,2048]{3,2,1,0:T(8,128)(2,1)S(1)}, u32[]{:S(2)}, u32[]{:S(2)}) async-start(bf16[4,1,72,2048]{3,2,1,0:T(8,128)(2,1)} %bitcast.295), calls=%async_computation.3 | async-start | bytes 2359296 | tf_op jit(solution)/shard_map/all_to_all | solution.py:186
  232.7 28.9 %reduce-scatter.3.cloned.1.call-done = bf16[128,2048]{1,0:T(8,128)(2,1)} async-done(((bf16[512,2048]{1,0:T(8,128)(2,1)}), bf16[128,2048]{1,0:T(8,128)(2,1)}) %reduce-scatter.3.cloned.1.call-update) | async-done | bytes 524304 | tf_op jit(solution)/shard_map/reduce_scatter | solution.py:170
  261.6 1.2 fusion.109
  262.8 2.0 fusion.111
  265.3 1.3 fusion.10
  (94 shorter events, 16.1 us)
Async XLA Ops:
  8.0 113.3 %copy-start = (bf16[1,512,2048]{2,1,0:T(8,128)(2,1)S(1)}, bf16[1,512,2048]{2,1,0:T(8,128)(2,1)}, u32[]{:S(2)}) copy-start(bf16[1,512,2048]{2,1,0:T(8,128)(2,1)} %param.33) | copy-start | bytes 6291460
  17.4 7.6 %copy-start.1 = (bf16[128,2048]{1,0:T(8,128)(2,1)S(1)}, bf16[128,2048]{1,0:T(8,128)(2,1)}, u32[]{:S(2)}) copy-start(bf16[128,2048]{1,0:T(8,128)(2,1)} %param.19) | copy-start | bytes 1572868
  17.4 7.8 %copy-start.2 = (f32[2048]{0:T(1024)S(1)}, f32[2048]{0:T(1024)}, u32[]{:S(2)}) copy-start(f32[2048]{0:T(1024)} %param.21) | copy-start | bytes 24580
  17.4 94.4 %all-to-all-start = ((bf16[16,1,72,2048]{3,2,1,0:T(8,128)(2,1)}), bf16[16,1,72,2048]{3,2,1,0:T(8,128)(2,1)}, u32[]{:S(2)}, u32[]{:S(2)}) async-start(bf16[16,1,72,2048]{3,2,1,0:T(8,128)(2,1)} %bitcast.285), calls=%async_computation.1 | async-start | bytes 9437184 | tf_op jit(solution)/shard_map/all_to_all | solution.py:149
  25.0 124.7 %all-gather.5.cloned.1.call-start = ((), (), s32[]{:S(2)}) async-start(), calls=%async_computation.5 | async-start | bytes 1310720 | tf_op jit(solution)/shard_map/all_gather | solution.py:101
  25.5 34.5 %collective-permute-start = (bf16[128,2048]{1,0:T(8,128)(2,1)S(1)}, bf16[128,2048]{1,0:T(8,128)(2,1)S(1)}, u32[]{:S(2)}, u32[]{:S(2)}) collective-permute-start(bf16[128,2048]{1,0:T(8,128)(2,1)S(1)} %fusion.108), channel_id=1, source_target_pairs={{0,1},{1,2},{2,3},{3,0},{4,5},{5,6},{6,7},{7,4},{8,9},{9,10},{10,1... | collective-permute-start | bytes 1572872 | tf_op jit(solution)/shard_map/ppermute | solution.py:47
  60.0 14.8 %collective-permute-start.1 = (bf16[128,2048]{1,0:T(8,128)(2,1)S(1)}, bf16[128,2048]{1,0:T(8,128)(2,1)}, u32[]{:S(2)}, u32[]{:S(2)}) collective-permute-start(bf16[128,2048]{1,0:T(8,128)(2,1)S(1)} %collective-permute-done), channel_id=1, source_target_pairs={{0,1},{1,2},{2,3},{3,0},{4,5},{5,6},{6,7},{7,4},{8,9},{9,10},{10,1... | collective-permute-start | bytes 1572872 | tf_op jit(solution)/shard_map/ppermute | solution.py:47
  74.7 10.6 %collective-permute-start.2 = (bf16[128,2048]{1,0:T(8,128)(2,1)}, bf16[128,2048]{1,0:T(8,128)(2,1)}, u32[]{:S(2)}, u32[]{:S(2)}) collective-permute-start(bf16[128,2048]{1,0:T(8,128)(2,1)} %collective-permute-done.1), channel_id=1, source_target_pairs={{0,1},{1,2},{2,3},{3,0},{4,5},{5,6},{6,7},{7,4},{8,9},{9,10},{10,1... | collective-permute-start | bytes 1572872 | tf_op jit(solution)/shard_map/ppermute | solution.py:47
  87.8 4.6 %copy-start.8 = (bf16[2048,256]{1,0:T(8,128)(2,1)S(1)}, bf16[2048,256]{1,0:T(8,128)(2,1)}, u32[]{:S(2)}) copy-start(bf16[2048,256]{1,0:T(8,128)(2,1)} %param.24) | copy-start | bytes 3145732
  90.3 2.1 copy-start.3
  92.4 1.5 copy-start.9
  93.8 71.7 %all-gather.3.cloned.1.call-start = ((), (), s32[]{:S(2)}) async-start(), calls=%async_computation.4 | async-start | bytes 1310720 | tf_op jit(solution)/shard_map/all_gather | solution.py:100
  96.9 131.1 %reduce-scatter.5.cloned.1.call-start = ((), (), s32[]{:S(2)}) async-start(), calls=%async_computation.7 | async-start | bytes 5898240 | tf_op jit(solution)/shard_map/reduce_scatter | solution.py:181
  111.8 3.7 %copy-start.7 = (bf16[1,2048,512]{2,1,0:T(8,128)(2,1)S(1)}, bf16[1,2048,512]{2,1,0:T(8,128)(2,1)}, u32[]{:S(2)}) copy-start(bf16[1,2048,512]{2,1,0:T(8,128)(2,1)} %param.31) | copy-start | bytes 6291460
  146.1 0.7 copy-start.4
  146.2 115.4 %reduce-scatter.3.cloned.1.call-start = ((), (), s32[]{:S(2)}) async-start(), calls=%async_computation.6 | async-start | bytes 2621440 | tf_op jit(solution)/shard_map/reduce_scatter | solution.py:170
  175.4 57.3 %copy-start.6 = (f32[128,2]{0,1:T(2,128)S(1)}, f32[128,2]{0,1:T(2,128)}, u32[]{:S(2)}) copy-start(f32[128,2]{0,1:T(2,128)} %param.30) | copy-start | bytes 3076
  175.4 87.5 %copy-start.5 = (f32[2048]{0:T(1024)S(1)}, f32[2048]{0:T(1024)}, u32[]{:S(2)}) copy-start(f32[2048]{0:T(1024)} %param.26) | copy-start | bytes 24580
  228.0 36.8 %all-to-all-start.1 = ((bf16[4,1,72,2048]{3,2,1,0:T(8,128)(2,1)}), bf16[4,1,72,2048]{3,2,1,0:T(8,128)(2,1)S(1)}, u32[]{:S(2)}, u32[]{:S(2)}) async-start(bf16[4,1,72,2048]{3,2,1,0:T(8,128)(2,1)} %bitcast.295), calls=%async_computation.3 | async-start | bytes 2359296 | tf_op jit(solution)/shard_map/all_to_all | solution.py:186
Sparse Core Ops, SparseCore 0:
  93.9 42.5 all-gather.4
  138.7 26.7 all-gather.2
Sparse Core Ops, SparseCore 1:
  146.3 81.7 reduce-scatter.4
  230.4 31.1 reduce-scatter.2
